TPU v7x, 32 devices: a whole 2x2x4 slice. The times are simulated.
32 devices in a mesh: sp: 8 (over z, x), tp: 4 (over y, core).
Axes of the slice: x: 2, y: 2, z: 4, core: 2. Of those that a mesh axis runs over, the one named last changes fastest.
Arguments:
- queries: bfloat16 [5120, 2048], P('sp', 'tp'), may hold values from -164 to 164
- keys: bfloat16 [5120, 512], P('sp', 'tp'), may hold values from -6 to 6
- values: bfloat16 [5120, 512], P('sp', 'tp'), may hold values from -6 to 6
- sink: float32 [32], P('tp'), may hold values from 4 to 8
- stream: bfloat16 [5120, 2048], P(('sp', 'tp')), may hold values from -6 to 6
- out_weight: bfloat16 [2048, 2048], P('tp'), may hold values from -0.5390625 to 0.5390625
- norm_gain: float32 [2048], replicated, may hold values from 0.1 to 1.9
- gate_weight: bfloat16 [2048, 5632], P('sp', 'tp'), may hold values from -0.125 to 0.125
- up_weight: bfloat16 [2048, 5632], P('sp', 'tp'), may hold values from -0.125 to 0.125
- down_weight: bfloat16 [5632, 2048], P('tp', 'sp'), may hold values from -0.23925781 to 0.23925781
Outputs:
- result: bfloat16 [5120, 2048], P(('sp', 'tp'))
All inputs are finite; a program needn't handle non-finite values.
Results may differ from a plain program's by a relative error of at most 0.019.
Values may be sent and summed in bfloat16 or wider, within the bound.
A program may use at most 128 MiB of HBM per device.

v0:
```python
import jax
import jax.numpy as jnp
from jax import lax
from jax.sharding import PartitionSpec as P

HEAD = 64
WINDOW = 128


def padded_2(cells, sides, width):
    for axis, dim in sides:
        count = lax.axis_size(axis)
        ends = count - 1
        head = lax.slice_in_dim(cells, 0, width, axis=dim)
        tail = lax.slice_in_dim(cells, cells.shape[dim] - width, cells.shape[dim], axis=dim)
        cells = jnp.concatenate(
            [
                lax.ppermute(tail, axis, [(i, (i + 1) % count) for i in range(ends)]),
                cells,
                lax.ppermute(head, axis, [((i + 1) % count, i) for i in range(ends)]),
            ],
            axis=dim,
        )
    return cells


def rotary(block, start):
    length = block.shape[0]
    middle = HEAD // 2
    inverse = 1.0 / 10000.0 ** (jnp.arange(0, HEAD, 2, dtype=jnp.float32) / HEAD)
    places = (start + jnp.arange(length, dtype=jnp.int32)).astype(jnp.float32)
    angles = places[:, None, None] * inverse[None, None, :]
    cosine_table = jnp.cos(angles)
    sine_table = jnp.sin(angles)
    pieces = block.astype(jnp.float32).reshape(length, -1, HEAD)
    leading = pieces[..., :middle]
    trailing = pieces[..., middle:]
    turned = jnp.concatenate(
        [
            leading * cosine_table - trailing * sine_table,
            trailing * cosine_table + leading * sine_table,
        ],
        -1,
    )
    return turned.reshape(length, -1).astype(jnp.bfloat16)


def window_attend(queries, keys, values, sink):
    rows_here = queries.shape[0]
    start = lax.axis_index("sp") * rows_here
    length = lax.axis_size("sp") * rows_here
    blocks = rows_here // WINDOW
    kv_width = keys.shape[1]
    kv_count = kv_width // HEAD
    head_count = queries.shape[1] // HEAD
    group = head_count // kv_count
    turned_q = rotary(queries, start)
    turned_k = rotary(keys, start)
    paired = jnp.concatenate([turned_k, values], 1)
    padded = padded_2(paired, (("sp", 0),), WINDOW)
    framed = padded.reshape(blocks + 2, WINDOW, 2 * kv_width)
    banded = jnp.concatenate([framed[:-2], framed[1:-1], framed[2:]], axis=1)
    key_band = banded[..., :kv_width].reshape(blocks, 3 * WINDOW, kv_count, HEAD)
    value_band = banded[..., kv_width:].reshape(blocks, 3 * WINDOW, kv_count, HEAD)
    query_blocks = turned_q.reshape(blocks, WINDOW, kv_count, group, HEAD)
    scores = jnp.einsum(
        "nqkgd,nskd->nkgqs", query_blocks, key_band, preferred_element_type=jnp.float32
    ) * HEAD ** (-0.5)
    query_place = (
        start + jnp.arange(blocks)[:, None, None] * WINDOW + jnp.arange(WINDOW)[None, :, None]
    )
    key_place = (
        start
        + jnp.arange(blocks)[:, None, None] * WINDOW
        - WINDOW
        + jnp.arange(3 * WINDOW)[None, None, :]
    )
    valid = (jnp.abs(key_place - query_place) <= WINDOW) & (key_place >= 0) & (key_place < length)
    scores = jnp.where(valid[:, None, None], scores, -jnp.inf)
    sink_grid = sink.reshape(kv_count, group)[None, :, :, None]
    top = jnp.maximum(jnp.max(scores, -1), sink_grid)
    raised = jnp.exp(scores - top[..., None])
    denom = jnp.sum(raised, -1) + jnp.exp(sink_grid - top)
    weights = (raised / denom[..., None]).astype(jnp.bfloat16)
    output = jnp.einsum(
        "nkgqs,nskd->nqkgd", weights, value_band, preferred_element_type=jnp.float32
    )
    return output.astype(jnp.bfloat16).reshape(rows_here, head_count * HEAD)


def collect_weights(gate_weight, up_weight, down_weight):
    return (
        lax.all_gather(gate_weight, "sp", axis=0, tiled=True),
        lax.all_gather(up_weight, "sp", axis=0, tiled=True),
        lax.all_gather(down_weight, "sp", axis=1, tiled=True),
    )


def local(
    queries, keys, values, sink, stream, out_weight, norm_gain, gate_weight, up_weight, down_weight
):
    attended = window_attend(queries, keys, values, sink)
    gathered = collect_weights(gate_weight, up_weight, down_weight)
    gate_whole, up_whole, down_whole = gathered
    rows = attended
    projected = lax.psum_scatter(
        jnp.dot(rows, out_weight, preferred_element_type=jnp.float32),
        "tp",
        scatter_dimension=0,
        tiled=True,
    )
    mixed = (stream.astype(jnp.float32) + projected).astype(jnp.bfloat16)
    mixed_wide = mixed.astype(jnp.float32)
    scale = lax.rsqrt(jnp.mean(mixed_wide * mixed_wide, -1, keepdims=True) + 1e-06)
    normed = (mixed_wide * scale * norm_gain).astype(jnp.bfloat16)
    piece = lax.all_gather(normed, "tp", axis=0, tiled=True)
    gate = jnp.dot(piece, gate_whole, preferred_element_type=jnp.float32)
    upward = jnp.dot(piece, up_whole, preferred_element_type=jnp.float32)
    hidden = (jax.nn.silu(gate) * upward).astype(jnp.bfloat16)
    rows = hidden
    lowered = lax.psum_scatter(
        jnp.dot(rows, down_whole, preferred_element_type=jnp.float32).astype(jnp.bfloat16),
        "tp",
        scatter_dimension=0,
        tiled=True,
    ).astype(jnp.float32)
    return (mixed_wide + 0.5 * lowered).astype(jnp.bfloat16)


def solution(mesh):
    placed = (
        P("sp", "tp"),
        P("sp", "tp"),
        P("sp", "tp"),
        P("tp"),
        P(("sp", "tp"), None),
        P("tp", None),
        P(),
        P("sp", "tp"),
        P("sp", "tp"),
        P("tp", "sp"),
    )
    return jax.shard_map(
        local, mesh=mesh, in_specs=placed, out_specs=P(("sp", "tp"), None), check_vma=False
    )
```

profile of v0, /device:TPU:0, one launch (start us, length us, event | category | flops | bytes accessed | tf_op | source)
XLA Modules:
  0.0 420.8 jit_solution(13338107045309871906)
XLA Ops:
  10.9 5.5 %collective-permute-start = (bf16[128,256]{0,1:T(8,128)(2,1)}, bf16[128,256]{0,1:T(8,128)(2,1)}, u32[]{:S(2)}, u32[]{:S(2)}) collective-permute-start(bf16[128,256]{0,1:T(8,128)(2,1)} %get-tuple-element.16), channel_id=1, source_target_pairs={{0,4},{4,8},{8,12},{12,16},{16,20},{20,24},{24,28},{1,5},{5,9},{9,... | collective-permute-start | bytes 196616 | tf_op jit(solution)/shard_map/ppermute | solution.py:18
  16.4 1.3 collective-permute-start.1
  17.9 1.4 copy.31
  21.6 1.8 convert_element_type.55
  23.4 1.3 max.17
  24.8 2.1 pad_maximum_fusion.5
  26.8 1.9 copy.26
  28.7 1.9 copy.27
  30.6 1.9 copy.28
  34.9 2.0 copy.30
  36.9 2.3 fusion.1
  39.3 1.9 fusion
  42.6 5.4 %fusion.9 = bf16[5,128,2,4,64]{1,4,3,2,0:T(8,128)(2,1)S(1)} fusion(bf16[5,384,2,64,1]{1,3,4,2,0:T(8,128)(2,1)S(1)} %bitcast.59, f32[5,2,384,128,4]{3,2,4,1,0:T(8,128)} %copy-done.1, f32[5,2,4,128]{3,2,1,0:T(4,128)S(1)} %exponential_add_fusion, f32[5,2,4,128]{3,2,1,0:T(4,128)S(1)} %broadcast_maximum_fusion, pred[5,128,384]{1,2,0:T(8,128)(4,1)S(1)} %fusion.11), kind=kOutput, calls=%fused_computation.18 | convolution fusion | flops 261816320 | bytes 9297920 | tf_op jit(solution)/shard_map/nkgqs,nskd->nqkgd/dot_general | solution.py:85
  48.5 4.0 fusion.12
  53.2 53.3 %reduce-scatter.3.cloned.1.call-done = f32[160,2048]{1,0:T(8,128)} async-done(((f32[640,2048]{1,0:T(8,128)}), f32[160,2048]{1,0:T(8,128)}) %reduce-scatter.3.cloned.1.call-update) | async-done | bytes 1310736 | tf_op jit(solution)/shard_map/reduce_scatter | solution.py:106
  106.4 1.6 fusion.5
  110.7 39.1 %all-gather.7.cloned.1.call-done = bf16[2048,1408]{1,0:T(8,128)(2,1)} async-done(((bf16[256,1408]{1,0:T(8,128)(2,1)}), bf16[2048,1408]{1,0:T(8,128)(2,1)}) %all-gather.7.cloned.1.call-update) | async-done | bytes 5767184 | tf_op jit(solution)/shard_map/all_gather | solution.py:93
  149.8 25.0 %all-gather.5.cloned.1.call-done = bf16[640,2048]{1,0:T(8,128)(2,1)} async-done(((bf16[160,2048]{1,0:T(8,128)(2,1)}), bf16[640,2048]{1,0:T(8,128)(2,1)}) %all-gather.5.cloned.1.call-update) | async-done | bytes 2621456 | tf_op jit(solution)/shard_map/all_gather | solution.py:116
  174.8 9.4 %fusion.25 = f32[640,1408]{1,0:T(8,128)} fusion(bf16[640,2048]{1,0:T(8,128)(2,1)} %all-gather.5.cloned.1.call-done, bf16[2048,1408]{1,0:T(8,128)(2,1)} %all-gather.7.cloned.1.call-done), kind=kOutput, calls=%fused_computation.62 | convolution fusion | flops 3690987520 | bytes 11993088 | tf_op jit(solution)/shard_map/dot_general | solution.py:117
  184.2 85.4 %all-gather.11.cloned.1.call-done = bf16[1408,2048]{1,0:T(8,128)(2,1)} async-done(((bf16[1408,256]{1,0:T(8,128)(2,1)}), bf16[1408,2048]{1,0:T(8,128)(2,1)}) %all-gather.11.cloned.1.call-update) | async-done | bytes 5767184 | tf_op jit(solution)/shard_map/all_gather | solution.py:95
  269.6 92.5 %all-gather.9.cloned.1.call-done = bf16[2048,1408]{1,0:T(8,128)(2,1)} async-done(((bf16[256,1408]{1,0:T(8,128)(2,1)}), bf16[2048,1408]{1,0:T(8,128)(2,1)}) %all-gather.9.cloned.1.call-update) | async-done | bytes 5767184 | tf_op jit(solution)/shard_map/all_gather | solution.py:94
  362.1 16.1 %convolution_convert_fusion = bf16[640,2048]{1,0:T(8,128)(2,1)} fusion(bf16[1408,2048]{1,0:T(8,128)(2,1)} %all-gather.11.cloned.1.call-done, bf16[640,2048]{1,0:T(8,128)(2,1)} %all-gather.5.cloned.1.call-done, bf16[2048,1408]{1,0:T(8,128)(2,1)} %all-gather.9.cloned.1.call-done, f32[640,1408]{1,0:T(8,128)} %fusion.25), kind=kOutput, calls=%fused_computation.8 | convolution fusion | flops 7388692480 | bytes 20381696 | tf_op jit(solution)/shard_map/dot_general | solution.py:122
  378.3 32.8 %reduce-scatter.5.cloned.1.call-done = bf16[160,2048]{1,0:T(8,128)(2,1)} async-done(((bf16[640,2048]{1,0:T(8,128)(2,1)}), bf16[160,2048]{1,0:T(8,128)(2,1)}) %reduce-scatter.5.cloned.1.call-update) | async-done | bytes 655376 | tf_op jit(solution)/shard_map/reduce_scatter | solution.py:121
  411.1 2.1 fusion.8
  (53 shorter events, 13.7 us)
Async XLA Ops:
  7.4 41.2 %copy-start = (bf16[512,2048]{1,0:T(8,128)(2,1)S(1)}, bf16[512,2048]{1,0:T(8,128)(2,1)}, u32[]{:S(2)}) copy-start(bf16[512,2048]{1,0:T(8,128)(2,1)} %param.15) | copy-start | bytes 6291460
  7.4 99.1 %reduce-scatter.3.cloned.1.call-start = ((), (), s32[]{:S(2)}) async-start(), calls=%async_computation.2 | async-start | bytes 6553600 | tf_op jit(solution)/shard_map/reduce_scatter | solution.py:106
  10.2 7.6 %copy-start.3 = (bf16[640,2,64]{0,2,1:T(8,128)(2,1)}, bf16[640,2,64]{0,2,1:T(8,128)(2,1)S(1)}, u32[]{:S(2)}) copy-start(bf16[640,2,64]{0,2,1:T(8,128)(2,1)S(1)} %pad_maximum_fusion.7) | copy-start | bytes 491524
  10.9 13.9 %collective-permute-start = (bf16[128,256]{0,1:T(8,128)(2,1)}, bf16[128,256]{0,1:T(8,128)(2,1)}, u32[]{:S(2)}, u32[]{:S(2)}) collective-permute-start(bf16[128,256]{0,1:T(8,128)(2,1)} %get-tuple-element.16), channel_id=1, source_target_pairs={{0,4},{4,8},{8,12},{12,16},{16,20},{20,24},{24,28},{1,5},{5,9},{9,... | collective-permute-start | bytes 196616 | tf_op jit(solution)/shard_map/ppermute | solution.py:18
  16.4 8.4 %collective-permute-start.1 = (bf16[128,256]{0,1:T(8,128)(2,1)}, bf16[128,256]{0,1:T(8,128)(2,1)}, u32[]{:S(2)}, u32[]{:S(2)}) collective-permute-start(bf16[128,256]{0,1:T(8,128)(2,1)} %get-tuple-element.17), channel_id=1, source_target_pairs={{4,0},{8,4},{12,8},{16,12},{20,16},{24,20},{28,24},{5,1},{9,5},{13... | collective-permute-start | bytes 196616 | tf_op jit(solution)/shard_map/ppermute | solution.py:20
  36.9 2.3 copy-start.6
  39.2 3.1 copy-start.1
  39.3 3.0 copy-start.2
  52.5 53.9 %copy-start.4 = (bf16[160,2048]{1,0:T(8,128)(2,1)S(1)}, bf16[160,2048]{1,0:T(8,128)(2,1)}, u32[]{:S(2)}) copy-start(bf16[160,2048]{1,0:T(8,128)(2,1)} %param.14) | copy-start | bytes 1966084
  52.5 55.5 %copy-start.5 = (f32[2048]{0:T(1024)S(1)}, f32[2048]{0:T(1024)}, u32[]{:S(2)}) copy-start(f32[2048]{0:T(1024)} %param.16) | copy-start | bytes 24580
  52.5 97.2 %all-gather.7.cloned.1.call-start = ((), (), s32[]{:S(2)}) async-start(), calls=%async_computation.4 | async-start | bytes 6488064 | tf_op jit(solution)/shard_map/all_gather | solution.py:93
  53.1 121.7 %all-gather.5.cloned.1.call-start = ((), (), s32[]{:S(2)}) async-start(), calls=%async_computation.3 | async-start | bytes 3276800 | tf_op jit(solution)/shard_map/all_gather | solution.py:116
  109.1 160.5 %all-gather.11.cloned.1.call-start = ((), (), s32[]{:S(2)}) async-start(), calls=%async_computation.6 | async-start | bytes 6488064 | tf_op jit(solution)/shard_map/all_gather | solution.py:95
  109.7 252.4 %all-gather.9.cloned.1.call-start = ((), (), s32[]{:S(2)}) async-start(), calls=%async_computation.5 | async-start | bytes 6488064 | tf_op jit(solution)/shard_map/all_gather | solution.py:94
  110.4 300.6 %reduce-scatter.5.cloned.1.call-start = ((), (), s32[]{:S(2)}) async-start(), calls=%async_computation.7 | async-start | bytes 3276800 | tf_op jit(solution)/shard_map/reduce_scatter | solution.py:121
Sparse Core Ops, SparseCore 0:
  52.7 53.7 reduce-scatter.2
  378.4 32.6 reduce-scatter.4
Sparse Core Ops, SparseCore 1:
  55.2 94.5 all-gather.6
  151.2 23.5 all-gather.4
  176.7 92.8 all-gather.10
  271.8 90.3 all-gather.8
where the time goes:
time: 421 us
  waiting for transfers between devices  330 us (78%)
  matrix products  37.2 us (9%)
  local copies, waits for them, and re-layouts  17.4 us (4%)
  between operations  15.2 us (4%)
  other arithmetic  13.9 us (3%)
  starting transfers between devices  7.16 us (2%)
    all_gather x1, waiting for transfers between devices, collect_weights(): lax.all_gather(up_weight, 'sp', axis=0, tiled=True)  92.5 us
    all_gather x1, waiting for transfers between devices, collect_weights(): lax.all_gather(down_weight, 'sp', axis=1, tiled=True)  85.4 us
    reduce_scatter x1, waiting for transfers between devices, local(): lax.psum_scatter(jnp.dot(rows, out_weight, preferred_element_type=jnp.flo...  53.3 us
    all_gather x1, waiting for transfers between devices, collect_weights(): lax.all_gather(gate_weight, 'sp', axis=0, tiled=True)  39.1 us
    reduce_scatter x1, waiting for transfers between devices, local(): lax.psum_scatter(jnp.dot(rows, down_whole, preferred_element_type=jnp.flo...  32.8 us
    all_gather x1, waiting for transfers between devices, local(): piece = lax.all_gather(normed, 'tp', axis=0, tiled=True)  25 us
    dot_general x1, matrix products, local(): jnp.dot(rows, down_whole, preferred_element_type=jnp.float32)  16.1 us
    dot_general x1, matrix products, local(): gate = jnp.dot(piece, gate_whole, preferred_element_type=jnp.float32)  9.43 us
  transfers between devices with their start and end apart: 8, of which 6 were waited for; matrix products, arithmetic and copies ran while one was open for 5% of the time, Pallas kernels for 0%

commit v1 on v0

--- a/solution.py
+++ b/solution.py
@@ -1,10 +1,18 @@
+import functools
+
 import jax
 import jax.numpy as jnp
 from jax import lax
+from jax.experimental import pallas as pl
+from jax.experimental.pallas import tpu as pltpu
 from jax.sharding import PartitionSpec as P
 
 HEAD = 64
 WINDOW = 128
+LANES = 128
+BF = jnp.bfloat16
+F32 = jnp.float32
+MESH = pl.DeviceIdType.MESH
 
 
 def padded_2(cells, sides, width):
@@ -127,6 +135,408 @@
     return (mixed_wide + 0.5 * lowered).astype(jnp.bfloat16)
 
 
+def turned(block, start):
+    length, width = block.shape
+    middle = HEAD // 2
+    inverse = 1.0 / 10000.0 ** (jnp.arange(0, HEAD, 2, dtype=F32) / HEAD)
+    places = (start + jnp.arange(length, dtype=jnp.int32)).astype(F32)
+    angles = places[:, None] * inverse[None, :]
+    cosine, sine = jnp.cos(angles), jnp.sin(angles)
+    heads = width // HEAD
+    cosine = jnp.tile(jnp.concatenate([cosine, cosine], 1), (1, heads))
+    sine = jnp.tile(jnp.concatenate([-sine, sine], 1), (1, heads))
+    cells = block.astype(F32)
+    ahead = jnp.roll(cells, -middle, 1)
+    behind = jnp.roll(cells, middle, 1)
+    lower = (jnp.arange(width) % HEAD < middle)[None]
+    return (cells * cosine + jnp.where(lower, ahead, behind) * sine).astype(BF)
+
+
+def layer_kernel(
+    dims, q_ref, kv_ref, sink_ref, stream_ref, w_ref, gain_ref, gu_own, gu_send, d_own, d_send,
+    out_ref,
+    kv, att, near, far, p_send, p_recv, kept, y_send, y_recv, mixed, na, nb, gu, dn,
+    hid, c_send, c_recv, acc, s1a, r1a, s1b, r1b, s2a, r2a, s2b, r2b,
+    gu_rs, d_rs, z_ss, x_ss, h_ss, h_rs, p_ss, p_rs, n_ss, n_rs, e_ss, e_rs,
+):
+    length, tokens, rows, per, tail, total = dims
+    s = lax.axis_index("sp")
+    z, x = s // 2, s % 2
+    t = lax.axis_index("tp")
+    y, c = t // 2, t % 2
+    across = s + 1 - 2 * x
+    at_x = {"sp": across}
+    at_y = {"tp": t + 2 - 4 * y}
+    at_c = {"tp": t + 1 - 2 * c}
+    has_up, has_down = z < length - 1, z > 0
+    last = 2 * length - 1
+
+    def send(src, dst, ssem, rsem, to):
+        return pltpu.make_async_remote_copy(
+            src_ref=src, dst_ref=dst, send_sem=ssem, recv_sem=rsem,
+            device_id=to, device_id_type=MESH,
+        )
+
+    barrier = pltpu.get_barrier_semaphore()
+
+    def greet(to):
+        pl.semaphore_signal(barrier, inc=1, device_id=to, device_id_type=MESH)
+
+    greet(at_x)
+    greet(at_y)
+    greet(at_c)
+    pl.when(has_up)(lambda: greet({"sp": s + 2}))
+    pl.when(has_down)(lambda: greet({"sp": s - 2}))
+    hop_up = (x == 1) & has_up
+    hop_down = (x == 0) & has_down
+    pl.when(hop_up)(lambda: greet({"sp": s + 1}))
+    pl.when(hop_down)(lambda: greet({"sp": s - 1}))
+    count = 3 + has_up.astype(jnp.int32) + has_down.astype(jnp.int32)
+    count = count + hop_up.astype(jnp.int32) + hop_down.astype(jnp.int32)
+    pl.semaphore_wait(barrier, count)
+
+    after = send(kv_ref.at[pl.ds(tokens - WINDOW, WINDOW)], kv.at[pl.ds(0, WINDOW)], h_ss.at[0], h_rs.at[0], {"sp": s + 1})
+    before = send(kv_ref.at[pl.ds(0, WINDOW)], kv.at[pl.ds(tokens + WINDOW, WINDOW)], h_ss.at[1], h_rs.at[1], {"sp": s - 1})
+    pl.when(s < last)(after.start)
+    pl.when(s > 0)(before.start)
+
+    x_gu = send(gu_send, gu.at[s], x_ss.at[0], gu_rs.at[s], at_x)
+    x_d = send(d_send, dn.at[s], x_ss.at[1], d_rs.at[s], at_x)
+    x_gu.start()
+
+    def line(kind, src, slot, index, side, way):
+        buf, sems = ((gu, gu_rs), (dn, d_rs))[kind]
+        to = {"sp": s + 2} if way == 0 else {"sp": s - 2}
+        return send(src, buf.at[slot], z_ss.at[kind, way, index, side], sems.at[slot], to)
+
+    def at_index(index):
+        if index == 0:
+            return z
+        tables = ((0, 1, 2, 3), (1, 0, 2, 3), (2, 3, 1, 0), (3, 2, 1, 0))
+        place = jnp.int32(tables[length - 1][index])
+        for k in range(length - 1):
+            place = jnp.where(z == k, tables[k][index], place)
+        return place
+
+    def landed(kind, slot):
+        buf, sems = ((gu, gu_rs), (dn, d_rs))[kind]
+        send(buf.at[slot], buf.at[slot], x_ss.at[0], sems.at[slot], at_x).wait_recv()
+
+    def ways(index):
+        if index == 0:
+            return (has_up, has_down)
+        place = at_index(index)
+        return ((place < z) & has_up, (place > z) & has_down)
+
+    def slot_of(index, side):
+        return 2 * at_index(index) + (x if side == 0 else 1 - x)
+
+    def push(kind, index, side):
+        slot = slot_of(index, side)
+        own = index == 0 and side == 0
+        buf = (gu, dn)[kind]
+        if not own:
+            landed(kind, slot)
+        src = (gu_own, d_own)[kind] if own else buf.at[slot]
+        for way, cond in enumerate(ways(index)):
+            pl.when(cond)(line(kind, src, slot, index, side, way).start)
+
+    push(0, 0, 0)
+    x_d.start()
+    kv[pl.ds(WINDOW, tokens), :] = kv_ref[...]
+    gu[s] = gu_own[...]
+    dn[s] = d_own[...]
+
+    @pl.when(s == 0)
+    def _():
+        kv[pl.ds(0, WINDOW), :] = jnp.zeros((WINDOW, kv.shape[1]), BF)
+
+    @pl.when(s == last)
+    def _():
+        kv[pl.ds(tokens + WINDOW, WINDOW), :] = jnp.zeros((WINDOW, kv.shape[1]), BF)
+
+    pl.when(s > 0)(after.wait_recv)
+    pl.when(s < last)(before.wait_recv)
+
+    kv_width = kv.shape[1] // 2
+    heads = q_ref.shape[1] // HEAD
+    group = heads // (kv_width // HEAD)
+
+    def attend(n, carry):
+        base = pl.multiple_of(n * WINDOW, WINDOW)
+        shape = (WINDOW, 3 * WINDOW)
+        q_at = lax.broadcasted_iota(jnp.int32, shape, 0)
+        k_at = lax.broadcasted_iota(jnp.int32, shape, 1) - WINDOW
+        place = k_at + (s * tokens + base)
+        valid = (jnp.abs(k_at - q_at) <= WINDOW) & (place >= 0) & (place < total)
+        outs = []
+        for h in range(heads):
+            g = h // group
+            q = q_ref[pl.ds(base, WINDOW), h * HEAD : (h + 1) * HEAD]
+            k = kv[pl.ds(base, 3 * WINDOW), g * HEAD : (g + 1) * HEAD]
+            v = kv[pl.ds(base, 3 * WINDOW), kv_width + g * HEAD : kv_width + (g + 1) * HEAD]
+            sc = lax.dot_general(q, k, (((1,), (1,)), ((), ())), preferred_element_type=F32)
+            sc = jnp.where(valid, sc * HEAD ** (-0.5), -jnp.inf)
+            sink = sink_ref[h]
+            top = jnp.maximum(jnp.max(sc, -1, keepdims=True), sink)
+            raised = jnp.exp(sc - top)
+            denom = jnp.sum(raised, -1, keepdims=True) + jnp.exp(sink - top)
+            weights = (raised / denom).astype(BF)
+            outs.append(jnp.dot(weights, v, preferred_element_type=F32).astype(BF))
+            if h % 2:
+                att[pl.ds(base, WINDOW), (h - 1) * HEAD : (h + 1) * HEAD] = jnp.concatenate(outs[-2:], 1)
+        return carry
+
+    blocks = tokens // WINDOW
+    lax.fori_loop(0, blocks - 1, attend, 0)
+    push(0, 0, 1)
+    lax.fori_loop(blocks - 1, blocks, attend, 0)
+
+    for dy in range(2):
+        yy = y if dy == 0 else 1 - y
+        mine = pl.multiple_of((2 * yy + c) * rows, 32)
+        theirs = pl.multiple_of((2 * yy + 1 - c) * rows, 32)
+        near[pl.ds(dy * rows, rows), :] = att[pl.ds(mine, rows), :]
+        far[pl.ds(dy * rows, rows), :] = att[pl.ds(theirs, rows), :]
+    model = out_ref.shape[1]
+    step = 4 * LANES
+
+    def project_far(n, carry):
+        cols = pl.ds(pl.multiple_of(n * step, step), step)
+        p_send[:, cols] = jnp.dot(far[...], w_ref[:, cols], preferred_element_type=F32).astype(BF)
+        return carry
+
+    def project_near(n, carry):
+        cols = pl.ds(pl.multiple_of(n * step, step), step)
+        kept[:, cols] = jnp.dot(near[...], w_ref[:, cols], preferred_element_type=F32)
+        return carry
+
+    lax.fori_loop(0, model // step, project_far, 0)
+    by_core = send(p_send, p_recv, p_ss.at[0], p_rs.at[0], at_c)
+    by_core.start()
+    lax.fori_loop(0, model // step, project_near, 0)
+    push(0, 1, 0)
+    by_core.wait_recv()
+    y_send[...] = (kept[rows:, :] + p_recv[rows:, :].astype(F32)).astype(BF)
+    by_y = send(y_send, y_recv, p_ss.at[1], p_rs.at[1], at_y)
+    by_y.start()
+    by_y.wait_recv()
+    mix = stream_ref[...].astype(F32) + (kept[:rows, :] + p_recv[:rows, :].astype(F32) + y_recv[...].astype(F32))
+    mix = mix.astype(BF)
+    mixed[...] = mix
+    wide = mix.astype(F32)
+    scale = lax.rsqrt(jnp.mean(wide * wide, -1, keepdims=True) + 1e-06)
+    normed = (wide * scale * gain_ref[...]).astype(BF)
+    cut = model // 2
+    na[0, 0] = normed[:, :cut]
+    nb[0, 0] = normed[:, cut:]
+
+    a_x = send(na.at[0, 0], na.at[0, 1], n_ss.at[0], n_rs.at[0], at_x)
+    b_y = send(nb.at[0, 0], nb.at[0, 2], n_ss.at[1], n_rs.at[1], at_y)
+    a_y0 = send(na.at[0, 0], na.at[0, 2], n_ss.at[2], n_rs.at[2], at_y)
+    a_y1 = send(na.at[0, 1], na.at[0, 3], n_ss.at[3], n_rs.at[3], at_y)
+    b_x0 = send(nb.at[0, 0], nb.at[0, 1], n_ss.at[4], n_rs.at[4], at_x)
+    b_x1 = send(nb.at[0, 2], nb.at[0, 3], n_ss.at[5], n_rs.at[5], at_x)
+    a_x.start()
+    b_y.start()
+    a_y0.start()
+    b_x0.start()
+    push(0, 1, 1)
+    a_x.wait_recv()
+    a_y1.start()
+    b_y.wait_recv()
+    b_x1.start()
+    push(0, 2, 0)
+    a_y0.wait_recv()
+    a_y1.wait_recv()
+    b_x0.wait_recv()
+    b_x1.wait_recv()
+    a_c = send(na.at[0], na.at[1], n_ss.at[6], n_rs.at[6], at_c)
+    b_c = send(nb.at[0], nb.at[1], n_ss.at[7], n_rs.at[7], at_c)
+    a_c.start()
+    b_c.start()
+    push(0, 2, 1)
+    push(1, 0, 0)
+    push(1, 0, 1)
+    for index in range(3, length):
+        push(0, index, 0)
+        push(0, index, 1)
+
+    def units(q, cols, size):
+        half = size // 2
+        depth = gu.shape[1]
+        lhs = na[q].reshape(4 * rows, cut)
+        rhs = nb[q].reshape(4 * rows, cut)
+        one = gu[pl.ds(0, length), :, cols].reshape(length * depth, size)
+        two = gu[pl.ds(length, length), :, cols].reshape(length * depth, size)
+        both = jnp.dot(lhs, one, preferred_element_type=F32) + jnp.dot(rhs, two, preferred_element_type=F32)
+        gate = both[:, :half]
+        return (gate / (1.0 + jnp.exp(-gate)) * both[:, half:]).astype(BF)
+
+    def hidden_of(q):
+        def body(n, carry):
+            cols = pl.ds(pl.multiple_of(n * 2 * LANES, 2 * LANES), 2 * LANES)
+            hid[q, :, pl.ds(pl.multiple_of(n * LANES, LANES), LANES)] = units(q, cols, 2 * LANES)
+            return carry
+
+        lax.fori_loop(0, per, body, 0)
+        hid[q, :, per * LANES :] = units(q, pl.ds(per * 2 * LANES, 2 * tail), 2 * tail)
+
+    hidden_of(0)
+    a_c.wait_recv()
+    b_c.wait_recv()
+    push(1, 1, 0)
+    push(1, 1, 1)
+    hidden_of(1)
+
+    part = d_own.shape[1]
+
+    def exchange(k, which):
+        src, dst, to = (
+            (c_send.at[k], c_recv.at[k], at_c),
+            (s1a.at[k], r1a.at[k], at_x),
+            (s1b.at[k], r1b.at[k], at_y),
+            (s2a.at[k], r2a.at[k], at_y),
+            (s2b.at[k], r2b.at[k], at_x),
+        )[which]
+        return send(src, dst, e_ss.at[which, k], e_rs.at[which, k], to)
+
+    def second(k):
+        exchange(k, 1).wait_recv()
+        exchange(k, 2).wait_recv()
+        a = [acc[k, 0, 2 * dy] + r1a[k, dy].astype(F32) for dy in range(2)]
+        b = [acc[k, 1, dx] + r1b[k, dx].astype(F32) for dx in range(2)]
+        s2a[k] = a[1].astype(BF)
+        s2b[k] = b[1].astype(BF)
+        exchange(k, 3).start()
+        exchange(k, 4).start()
+        acc[k, 0, 0] = a[0]
+        acc[k, 1, 0] = b[0]
+
+    for k in range(length):
+        if k > 1:
+            push(1, k, 0)
+            push(1, k, 1)
+        low = 2 * at_index(k)
+        for side in range(2):
+            weight = dn[low + side]
+            c_send[k, side] = jnp.dot(hid[1], weight, preferred_element_type=F32).astype(BF)
+        exchange(k, 0).start()
+        for side in range(2):
+            weight = dn[low + side]
+            acc[k, side] = jnp.dot(hid[0], weight, preferred_element_type=F32).reshape(4, rows, part)
+        if k:
+            second(k - 1)
+        exchange(k, 0).wait_recv()
+        acc[k] = acc[k] + c_recv[k].reshape(2, 4, rows, part).astype(F32)
+        for dy in range(2):
+            s1a[k, dy] = acc[k, 0, 2 * dy + 1].astype(BF)
+        for dx in range(2):
+            s1b[k, dx] = acc[k, 1, 2 + dx].astype(BF)
+        exchange(k, 1).start()
+        exchange(k, 2).start()
+    second(length - 1)
+    for k in range(length):
+        exchange(k, 3).wait_recv()
+        exchange(k, 4).wait_recv()
+        for side, got in ((0, r2a), (1, r2b)):
+            cols = pl.ds(pl.multiple_of((2 * at_index(k) + side) * part, part), part)
+            lowered = acc[k, side, 0] + got[k].astype(F32)
+            out_ref[:, cols] = (mixed[:, cols].astype(F32) + 0.5 * lowered).astype(BF)
+
+    pl.when(s < last)(after.wait_send)
+    pl.when(s > 0)(before.wait_send)
+    for copy in (x_gu, x_d, by_core, by_y, a_x, b_y, a_y0, a_y1, b_x0, b_x1, a_c, b_c):
+        copy.wait_send()
+    for k in range(length):
+        for which in range(5):
+            exchange(k, which).wait_send()
+    for kind in range(2):
+        for index in range(length):
+            for side in range(2):
+                slot = slot_of(index, side)
+                own = index == 0 and side == 0
+                src = (gu_own, d_own)[kind] if own else (gu, dn)[kind].at[slot]
+                for way, cond in enumerate(ways(index)):
+                    pl.when(cond)(line(kind, src, slot, index, side, way).wait_send)
+
+
+def local_lines(
+    queries, keys, values, sink, stream, out_weight, norm_gain, gate_weight, up_weight, down_weight
+):
+    length = lax.axis_size("sp") // 2
+    s = lax.axis_index("sp")
+    tokens = queries.shape[0]
+    rows, model = stream.shape
+    depth, wide = gate_weight.shape
+    per = wide // LANES // 2
+    tail = wide // 2 - per * LANES
+    half = wide // 2
+    edge = 2 * per * LANES
+
+    def pieces(x):
+        out = []
+        for n in range(per):
+            at = (x * per + n) * LANES
+            out += [gate_weight[:, at : at + LANES], up_weight[:, at : at + LANES]]
+        at = edge + x * tail
+        out += [gate_weight[:, at : at + tail], up_weight[:, at : at + tail]]
+        return jnp.concatenate(out, 1)
+
+    def lowers(x):
+        at = x * per * LANES
+        end = edge + x * tail
+        return jnp.concatenate([down_weight[at : at + per * LANES], down_weight[end : end + tail]], 0)
+
+    first = s % 2 == 0
+    gu_0, gu_1, d_0, d_1 = pieces(0), pieces(1), lowers(0), lowers(1)
+    paired = jnp.concatenate([turned(keys, s * tokens), values], 1)
+    part = down_weight.shape[1]
+    vmem = pl.BlockSpec(memory_space=pltpu.VMEM)
+    dma = pltpu.SemaphoreType.DMA
+    dims = (length, tokens, rows, per, tail, tokens * 2 * length)
+    return pl.pallas_call(
+        functools.partial(layer_kernel, dims),
+        out_shape=jax.ShapeDtypeStruct((rows, model), BF),
+        in_specs=[vmem, vmem, pl.BlockSpec(memory_space=pltpu.SMEM)] + [vmem] * 7,
+        out_specs=vmem,
+        scratch_shapes=[
+            pltpu.VMEM((tokens + 2 * WINDOW, paired.shape[1]), BF),
+            pltpu.VMEM(queries.shape, BF),
+            pltpu.VMEM((2 * rows, queries.shape[1]), BF),
+            pltpu.VMEM((2 * rows, queries.shape[1]), BF),
+            pltpu.VMEM((2 * rows, model), BF),
+            pltpu.VMEM((2 * rows, model), BF),
+            pltpu.VMEM((2 * rows, model), F32),
+            pltpu.VMEM((rows, model), BF),
+            pltpu.VMEM((rows, model), BF),
+            pltpu.VMEM((rows, model), BF),
+            pltpu.VMEM((2, 4, rows, model // 2), BF),
+            pltpu.VMEM((2, 4, rows, model // 2), BF),
+            pltpu.VMEM((2 * length, depth, 2 * half), BF),
+            pltpu.VMEM((2 * length, half, part), BF),
+            pltpu.VMEM((2, 4 * rows, half), BF),
+            pltpu.VMEM((length, 2, 4 * rows, part), BF),
+            pltpu.VMEM((length, 2, 4 * rows, part), BF),
+            pltpu.VMEM((length, 2, 4, rows, part), F32),
+        ]
+        + [pltpu.VMEM((length, 2, rows, part), BF)] * 4
+        + [pltpu.VMEM((length, rows, part), BF)] * 4
+        + [
+            dma((2 * length,)), dma((2 * length,)), dma((2, 2, length, 2)), dma((2,)),
+            dma((2,)), dma((2,)), dma((2,)), dma((2,)), dma((8,)), dma((8,)),
+            dma((5, length)), dma((5, length)),
+        ],
+        compiler_params=pltpu.CompilerParams(
+            collective_id=0, has_side_effects=True, vmem_limit_bytes=63 * 1024 * 1024
+        ),
+    )(
+        turned(queries, s * tokens), paired, sink, stream, out_weight, norm_gain[None],
+        jnp.where(first, gu_0, gu_1), jnp.where(first, gu_1, gu_0),
+        jnp.where(first, d_0, d_1), jnp.where(first, d_1, d_0),
+    )
+
+
 def solution(mesh):
     placed = (
         P("sp", "tp"),
@@ -140,6 +550,7 @@
         P("sp", "tp"),
         P("tp", "sp"),
     )
+    lines = mesh.shape["tp"] == 4 and mesh.shape["sp"] == 8
     return jax.shard_map(
-        local, mesh=mesh, in_specs=placed, out_specs=P(("sp", "tp"), None), check_vma=False
-    )
+        local_lines if lines else local, mesh=mesh, in_specs=placed, out_specs=P(("sp", "tp"), None), check_vma=False
+    )

time: 421 us -> 205 us (0.49)
  waiting for transfers between devices: 330 us -> 0 us
  Pallas kernels: 0 us -> 185 us
  matrix products: 37.2 us -> 0 us
  between operations: 15.2 us -> 0.18 us
  starting transfers between devices: 7.16 us -> 0 us
  other arithmetic: 13.9 us -> 7.14 us
  local copies, waits for them, and re-layouts: 17.4 us -> 12.2 us
    all_gather x4 -> x0, waiting for transfers between devices: 242 us -> none  [the longest x1 92.5 us: collect_weights(): lax.all_gather(up_weight, 'sp', axis=0, tiled=True)]
    pallas_call x0 -> x1, Pallas kernels: none -> 185 us  [local_lines(): pl.pallas_call(functools.partial(layer_kernel, dims), out_shape=jax.Shape...]
    reduce_scatter x2 -> x0, waiting for transfers between devices: 86.1 us -> none  [the longest x1 53.3 us: local(): lax.psum_scatter(jnp.dot(rows, out_weight, preferred_element_type=jnp.flo...]
    dot_general x5 -> x0, matrix products: 37.2 us -> none  [the longest x1 16.1 us: local(): jnp.dot(rows, down_whole, preferred_element_type=jnp.float32)]
    ppermute x2 -> x0, starting transfers between devices: 6.77 us -> none  [the longest x1 5.49 us: padded_2(): lax.ppermute(tail, axis, [(i, (i + 1) % count) for i in range(ends)])]
    another operation x0 -> x8, local copies, waits for them, and re-layouts: none -> 5.88 us  [the longest x4 4.12 us: turned(): cosine = jnp.tile(jnp.concatenate([cosine, cosine], 1), (1, heads))]
    slice x5 -> x9, local copies, waits for them, and re-layouts: 7.22 us -> 1.97 us  [the longest x4 1.55 us: turned(): behind = jnp.roll(cells, middle, 1)]
  transfers between devices with their start and end apart: 8 -> 0, of which waited for: 6 -> 0; matrix products, arithmetic and copies ran while one was open for 5% -> 0% of each run, Pallas kernels for 0% -> 0%
where the time goes in v1:
time: 205 us
  Pallas kernels  185 us (90%)
  local copies, waits for them, and re-layouts  12.2 us (6%)
  other arithmetic  7.14 us (3%)
    pallas_call x1, Pallas kernels, local_lines(): pl.pallas_call(functools.partial(layer_kernel, dims), out_shape=jax.Shape...  185 us
    another operation x4, local copies, waits for them, and re-layouts, turned(): cosine = jnp.tile(jnp.concatenate([cosine, cosine], 1), (1, heads))  4.12 us

profile of v1, /device:TPU:0, one launch (start us, length us, event | category | flops | bytes accessed | tf_op | source)
XLA Modules:
  0.0 204.6 jit_solution(15993914942797919390)
XLA Ops:
  0.0 0.4 multiply_cosine_fusion
  0.5 1.5 copy.12
  2.0 0.9 fusion.18
  2.9 0.4 fusion.19
  3.4 1.2 tile.16
  4.5 2.8 %copy.11 = f32[640,512]{1,0:T(8,128)} copy(f32[640,512]{0,1:T(8,128)} %bitcast.6) | data formatting | bytes 2621440 | tf_op jit(solution)/shard_map/tile | solution.py:146
  7.3 3.5 %fusion.2.q_ref = bf16[640,512]{1,0:T(8,128)(2,1)} fusion(f32[640,512]{1,0:T(8,128)} %copy.12, f32[640,32]{1,0:T(8,128)} %get-tuple-element.38, f32[640,480]{1,0:T(8,128)S(1)} %get-tuple-element.40, f32[640,480]{1,0:T(8,128)S(1)} %get-tuple-element.39, f32[640,32]{1,0:T(8,128)} %get-tuple-element.37, f32[640,512]{1,0:T(8,128)} %copy.11, ...), kind=kLoop, calls=%fused_computation.3 | loop fusion | flops 2621440 | bytes 6554112 | tf_op jit(solution)/shard_map/convert_element_type | solution.py:152
  10.8 0.2 copy.14
  11.0 0.7 copy-done.1
  11.7 0.1 fusion.20
  11.8 0.1 fusion.21
  11.9 0.2 copy.13
  12.1 0.2 fusion.5
  12.4 0.6 copy-done.7
  13.0 0.8 pad_maximum_fusion.2.kv_ref
  13.8 0.1 fusion.17
  13.9 0.4 copy-done.5
  14.3 0.1 fusion.16
  14.6 0.3 concatenate.47
  14.9 0.3 concatenate.46
  15.2 1.3 broadcast_select_fusion
  16.5 1.0 broadcast_select_fusion.2
  17.5 185.1 %shard_map.100 = bf16[160,2048]{1,0:T(8,128)(2,1)} custom-call(bf16[640,512]{1,0:T(8,128)(2,1)} %fusion.2.q_ref, bf16[640,256]{1,0:T(8,128)(2,1)} %pad_maximum_fusion.2.kv_ref, f32[8]{0:T(128)} %sink_ref.1, bf16[160,2048]{1,0:T(8,128)(2,1)} %stream_ref.1, bf16[512,2048]{1,0:T(8,128)(2,1)} %w_ref.1, f32[1,2048]{1,0:T(1,128)} %bitcast.9, ...), custom_call_target="tpu_custom_call" | custom-call | tf_op jit(solution)/shard_map/pallas_call | solution.py:498
  202.6 2.0 copy.16
  (24 shorter events, 0.4 us)
Async XLA Ops:
  0.4 1.6 copy-start.2
  0.5 1.5 copy-start
  7.3 3.5 %copy-start.3 = (f32[640,64]{0,1:T(8,128)S(1)}, f32[640,64]{0,1:T(8,128)}, u32[]{:S(2)}) copy-start(f32[640,64]{0,1:T(8,128)} %copy-done.2) | copy-start | bytes 491524
  10.8 0.9 copy-start.1
  12.1 0.9 copy-start.7
  12.1 1.7 copy-start.4
  13.0 1.3 copy-start.5
  15.2 1.3 copy-start.6

commit v2 on v1

--- a/solution.py
+++ b/solution.py
@@ -135,25 +135,27 @@
     return (mixed_wide + 0.5 * lowered).astype(jnp.bfloat16)
 
 
-def turned(block, start):
-    length, width = block.shape
-    middle = HEAD // 2
-    inverse = 1.0 / 10000.0 ** (jnp.arange(0, HEAD, 2, dtype=F32) / HEAD)
+def turn_tables(length, start):
+    lane = jnp.arange(LANES)
+    pair = (lane % (HEAD // 2)).astype(F32) * 2.0
+    inverse = 1.0 / 10000.0 ** (pair / HEAD)
     places = (start + jnp.arange(length, dtype=jnp.int32)).astype(F32)
     angles = places[:, None] * inverse[None, :]
-    cosine, sine = jnp.cos(angles), jnp.sin(angles)
-    heads = width // HEAD
-    cosine = jnp.tile(jnp.concatenate([cosine, cosine], 1), (1, heads))
-    sine = jnp.tile(jnp.concatenate([-sine, sine], 1), (1, heads))
+    side = jnp.where(lane % HEAD < HEAD // 2, -1.0, 1.0).astype(F32)
+    return jnp.cos(angles), jnp.sin(angles) * side[None, :]
+
+
+def turned(block, cosine, sine):
     cells = block.astype(F32)
-    ahead = jnp.roll(cells, -middle, 1)
-    behind = jnp.roll(cells, middle, 1)
-    lower = (jnp.arange(width) % HEAD < middle)[None]
-    return (cells * cosine + jnp.where(lower, ahead, behind) * sine).astype(BF)
+    lane = lax.broadcasted_iota(jnp.int32, cells.shape, 1)
+    ahead = pltpu.roll(cells, LANES - HEAD // 2, 1)
+    behind = pltpu.roll(cells, HEAD // 2, 1)
+    other = jnp.where(lane % HEAD < HEAD // 2, ahead, behind)
+    return (cells * cosine + other * sine).astype(BF)
 
 
 def layer_kernel(
-    dims, q_ref, kv_ref, sink_ref, stream_ref, w_ref, gain_ref, gu_own, gu_send, d_own, d_send,
+    dims, q_ref, kv_ref, cos_ref, sin_ref, sink_ref, stream_ref, w_ref, gain_ref, gu_own, gu_send, d_own, d_send,
     out_ref,
     kv, att, near, far, p_send, p_recv, kept, y_send, y_recv, mixed, na, nb, gu, dn,
     hid, c_send, c_recv, acc, s1a, r1a, s1b, r1b, s2a, r2a, s2b, r2b,
@@ -241,7 +243,16 @@
         for way, cond in enumerate(ways(index)):
             pl.when(cond)(line(kind, src, slot, index, side, way).start)
 
+    middle = has_up & has_down
+
+    def relay(kind, index, side):
+        pl.when(middle)(lambda: push(kind, index, side))
+
+    def settle(kind, index, side):
+        pl.when(jnp.logical_not(middle))(lambda: landed(kind, slot_of(index, side)))
+
     push(0, 0, 0)
+    push(1, 0, 0)
     x_d.start()
     kv[pl.ds(WINDOW, tokens), :] = kv_ref[...]
     gu[s] = gu_own[...]
@@ -260,6 +271,15 @@
 
     kv_width = kv.shape[1] // 2
     heads = q_ref.shape[1] // HEAD
+
+    def turn_keys(n, carry):
+        at = pl.ds(pl.multiple_of(n * WINDOW, WINDOW), WINDOW)
+        for p in range(kv_width // LANES):
+            cols = slice(p * LANES, (p + 1) * LANES)
+            kv[at, cols] = turned(kv[at, cols], cos_ref[at, :], sin_ref[at, :])
+        return carry
+
+    lax.fori_loop(0, tokens // WINDOW + 2, turn_keys, 0)
     group = heads // (kv_width // HEAD)
 
     def attend(n, carry):
@@ -272,7 +292,11 @@
         outs = []
         for h in range(heads):
             g = h // group
-            q = q_ref[pl.ds(base, WINDOW), h * HEAD : (h + 1) * HEAD]
+            if h % 2 == 0:
+                here = pl.ds(pl.multiple_of(base + WINDOW, WINDOW), WINDOW)
+                two = q_ref[pl.ds(base, WINDOW), h * HEAD : (h + 2) * HEAD]
+                two = turned(two, cos_ref[here, :], sin_ref[here, :])
+            q = two[:, HEAD * (h % 2) : HEAD * (h % 2 + 1)]
             k = kv[pl.ds(base, 3 * WINDOW), g * HEAD : (g + 1) * HEAD]
             v = kv[pl.ds(base, 3 * WINDOW), kv_width + g * HEAD : kv_width + (g + 1) * HEAD]
             sc = lax.dot_general(q, k, (((1,), (1,)), ((), ())), preferred_element_type=F32)
@@ -288,9 +312,22 @@
         return carry
 
     blocks = tokens // WINDOW
-    lax.fori_loop(0, blocks - 1, attend, 0)
-    push(0, 0, 1)
-    lax.fori_loop(blocks - 1, blocks, attend, 0)
+    def between(n, carry):
+        attend(n, carry)
+
+        @pl.when(n == blocks - 3)
+        def _():
+            push(0, 0, 1)
+
+        @pl.when(n == blocks - 2)
+        def _():
+            relay(0, 1, 0)
+            relay(0, 2, 0)
+
+        return carry
+
+    lax.fori_loop(0, blocks, between, 0)
+    push(1, 0, 1)
 
     for dy in range(2):
         yy = y if dy == 0 else 1 - y
@@ -315,11 +352,12 @@
     by_core = send(p_send, p_recv, p_ss.at[0], p_rs.at[0], at_c)
     by_core.start()
     lax.fori_loop(0, model // step, project_near, 0)
-    push(0, 1, 0)
     by_core.wait_recv()
     y_send[...] = (kept[rows:, :] + p_recv[rows:, :].astype(F32)).astype(BF)
     by_y = send(y_send, y_recv, p_ss.at[1], p_rs.at[1], at_y)
     by_y.start()
+    relay(0, 1, 1)
+    relay(0, 2, 1)
     by_y.wait_recv()
     mix = stream_ref[...].astype(F32) + (kept[:rows, :] + p_recv[:rows, :].astype(F32) + y_recv[...].astype(F32))
     mix = mix.astype(BF)
@@ -341,12 +379,11 @@
     b_y.start()
     a_y0.start()
     b_x0.start()
-    push(0, 1, 1)
+    relay(0, 3, 0)
     a_x.wait_recv()
     a_y1.start()
     b_y.wait_recv()
     b_x1.start()
-    push(0, 2, 0)
     a_y0.wait_recv()
     a_y1.wait_recv()
     b_x0.wait_recv()
@@ -355,12 +392,13 @@
     b_c = send(nb.at[0], nb.at[1], n_ss.at[7], n_rs.at[7], at_c)
     a_c.start()
     b_c.start()
-    push(0, 2, 1)
-    push(1, 0, 0)
-    push(1, 0, 1)
-    for index in range(3, length):
-        push(0, index, 0)
-        push(0, index, 1)
+    relay(0, 3, 1)
+    for index in (1, 2):
+        for side in range(2):
+            relay(1, index, side)
+    for index in range(1, length):
+        for side in range(2):
+            settle(0, index, side)
 
     def units(q, cols, size):
         half = size // 2
@@ -383,11 +421,11 @@
         hid[q, :, per * LANES :] = units(q, pl.ds(per * 2 * LANES, 2 * tail), 2 * tail)
 
     hidden_of(0)
+    relay(1, 3, 0)
     a_c.wait_recv()
     b_c.wait_recv()
-    push(1, 1, 0)
-    push(1, 1, 1)
     hidden_of(1)
+    relay(1, 3, 1)
 
     part = d_own.shape[1]
 
@@ -414,9 +452,9 @@
         acc[k, 1, 0] = b[0]
 
     for k in range(length):
-        if k > 1:
-            push(1, k, 0)
-            push(1, k, 1)
+        if k:
+            settle(1, k, 0)
+            settle(1, k, 1)
         low = 2 * at_index(k)
         for side in range(2):
             weight = dn[low + side]
@@ -490,7 +528,8 @@
 
     first = s % 2 == 0
     gu_0, gu_1, d_0, d_1 = pieces(0), pieces(1), lowers(0), lowers(1)
-    paired = jnp.concatenate([turned(keys, s * tokens), values], 1)
+    paired = jnp.concatenate([keys, values], 1)
+    cosine, sine = turn_tables(tokens + 2 * WINDOW, s * tokens - WINDOW)
     part = down_weight.shape[1]
     vmem = pl.BlockSpec(memory_space=pltpu.VMEM)
     dma = pltpu.SemaphoreType.DMA
@@ -498,7 +537,7 @@
     return pl.pallas_call(
         functools.partial(layer_kernel, dims),
         out_shape=jax.ShapeDtypeStruct((rows, model), BF),
-        in_specs=[vmem, vmem, pl.BlockSpec(memory_space=pltpu.SMEM)] + [vmem] * 7,
+        in_specs=[vmem] * 4 + [pl.BlockSpec(memory_space=pltpu.SMEM)] + [vmem] * 7,
         out_specs=vmem,
         scratch_shapes=[
             pltpu.VMEM((tokens + 2 * WINDOW, paired.shape[1]), BF),
@@ -531,7 +570,7 @@
             collective_id=0, has_side_effects=True, vmem_limit_bytes=63 * 1024 * 1024
         ),
     )(
-        turned(queries, s * tokens), paired, sink, stream, out_weight, norm_gain[None],
+        queries, paired, cosine, sine, sink, stream, out_weight, norm_gain[None],
         jnp.where(first, gu_0, gu_1), jnp.where(first, gu_1, gu_0),
         jnp.where(first, d_0, d_1), jnp.where(first, d_1, d_0),
     )

time: 205 us -> 178 us (0.87)
  Pallas kernels: 185 us -> 165 us
  local copies, waits for them, and re-layouts: 12.2 us -> 5.93 us
    pallas_call x1, Pallas kernels: 185 us -> 165 us  [local_lines(): pl.pallas_call(functools.partial(layer_kernel, dims), out_shape=jax.Shape...]
    another operation x8 -> x0, local copies, waits for them, and re-layouts: 5.88 us -> none  [the longest x4 4.12 us: turned(): cosine = jnp.tile(jnp.concatenate([cosine, cosine], 1), (1, heads))]
    convert_element_type x3 -> x1, other arithmetic: 3.7 us -> 0.01 us  [turn_tables(): places = (start + jnp.arange(length, dtype=jnp.int32)).astype(F32)]
    mul x0 -> x1, other arithmetic: none -> 2.62 us  [turn_tables(): return (jnp.cos(angles), jnp.sin(angles) * side[None, :])]
where the time goes in v2:
time: 178 us
  Pallas kernels  165 us (93%)
  other arithmetic  6.66 us (4%)
  local copies, waits for them, and re-layouts  5.93 us (3%)
    pallas_call x1, Pallas kernels, local_lines(): pl.pallas_call(functools.partial(layer_kernel, dims), out_shape=jax.Shape...  165 us

profile of v2, /device:TPU:0, one launch (start us, length us, event | category | flops | bytes accessed | tf_op | source)
XLA Modules:
  0.0 177.9 jit_solution(10282212328849217)
XLA Ops:
  0.0 0.0 copy-start
  0.0 0.8 fusion.6
  0.9 1.0 fusion.7
  1.9 1.8 pad_maximum_fusion.2.kv_ref
  3.7 0.0 copy-start.1
  3.7 1.2 fusion.5
  4.9 1.0 broadcast_select_fusion.2
  5.9 0.0 copy-done
  5.9 0.1 fusion.10
  6.0 0.0 copy-done.1
  6.0 0.1 fusion.9
  6.2 0.3 concatenate.17
  6.5 0.3 concatenate.16
  6.8 1.3 broadcast_select_fusion
  8.1 2.6 %fusion = (f32[896,128]{1,0:T(8,128)}, f32[896,128]{1,0:T(8,128)}) fusion(f32[128]{0:T(128)S(1)} %get-tuple-element.39, f32[128]{0:T(128)S(1)} %get-tuple-element.40, f32[896]{0:T(1024)S(1)} %add_convert_fusion), kind=kLoop, calls=%fused_computation.4 | loop fusion | flops 229376 | bytes 922112 | tf_op jit(solution)/shard_map/mul | solution.py:145
  10.7 165.2 %shard_map.100 = bf16[160,2048]{1,0:T(8,128)(2,1)} custom-call(bf16[640,512]{1,0:T(8,128)(2,1)} %q_ref.1, bf16[640,256]{1,0:T(8,128)(2,1)} %pad_maximum_fusion.2.kv_ref, f32[896,128]{1,0:T(8,128)} %get-tuple-element.38.cos_ref, f32[896,128]{1,0:T(8,128)} %get-tuple-element.37.sin_ref, f32[8]{0:T(128)} %sink_ref.1, bf16[160,2048]{1,0:T(8,128)(2,1)} %stream_ref.1, ...), custom_call_target="tpu_custom_call" | custom-call | tf_op jit(solution)/shard_map/pallas_call | solution.py:537
  175.9 2.0 %copy.12 = bf16[160,2048]{1,0:T(8,128)(2,1)} copy(bf16[160,2048]{1,0:T(8,128)(2,1)} %shard_map.100) | data formatting | bytes 1310720
  (2 shorter events, 0.0 us)
Async XLA Ops:
  0.0 5.9 %copy-start = (bf16[256,1408]{1,0:T(8,128)(2,1)S(1)}, bf16[256,1408]{1,0:T(8,128)(2,1)}, u32[]{:S(2)}) copy-start(bf16[256,1408]{1,0:T(8,128)(2,1)} %param.17) | copy-start | bytes 2162692
  3.7 2.3 %copy-start.1 = (bf16[256,1408]{1,0:T(8,128)(2,1)S(1)}, bf16[256,1408]{1,0:T(8,128)(2,1)}, u32[]{:S(2)}) copy-start(bf16[256,1408]{1,0:T(8,128)(2,1)} %param.18) | copy-start | bytes 2162692
